TPU v7x, 32 devices: a whole 2x2x4 slice. The times are simulated.
32 devices in a mesh: grp: 2 (over x), kv: 4 (over z), tp: 4 (over y, core).
Axes of the slice: x: 2, y: 2, z: 4, core: 2. Of those that a mesh axis runs over, the one named last changes fastest.
Arguments:
- stream: bfloat16 [32, 4096], P('grp', ('kv', 'tp')), parts along dimension 0, may hold values from -6 to 6
- attn_gain: bfloat16 [4096], P('kv'), may hold values from 0.099609375 to 1.8984375
- mlp_gain: bfloat16 [4096], P('kv'), may hold values from 0.099609375 to 1.8984375
- w_query: bfloat16 [4096, 4096], P('kv', 'tp'), may hold values from -0.09375 to 0.09375
- w_key: bfloat16 [4096, 4096], P('kv', 'tp'), may hold values from -0.09375 to 0.09375
- w_value: bfloat16 [4096, 4096], P('kv', 'tp'), may hold values from -0.09375 to 0.09375
- w_zgate: bfloat16 [4096, 4096], P('kv', 'tp'), may hold values from -0.09375 to 0.09375
- w_decay: bfloat16 [4096, 32], P('kv'), may hold values from -0.09375 to 0.09375
- w_beta: bfloat16 [4096, 32], P('kv'), may hold values from -0.09375 to 0.09375
- decay_rate: float32 [32], P('tp'), may hold values from 0.03 to 3
- head_gain: float32 [128], replicated, may hold values from 0.1 to 1.9
- w_attn_out: bfloat16 [4096, 4096], P('tp', 'kv'), may hold values from -0.09375 to 0.09375
- w_gate: bfloat16 [4096, 11264], P('kv', 'tp'), may hold values from -0.09375 to 0.09375
- w_up: bfloat16 [4096, 11264], P('kv', 'tp'), may hold values from -0.09375 to 0.09375
- w_down: bfloat16 [11264, 4096], P('tp', 'kv'), may hold values from -0.0546875 to 0.0546875
- state: float32 [32, 32, 128, 128], P(('grp', 'kv'), 'tp'), parts along dimension 0, may hold values from -4 to 4
Outputs:
- next_stream: bfloat16 [32, 4096], P('grp', ('kv', 'tp')), parts along dimension 0
- new_state: float32 [32, 32, 128, 128], P(('grp', 'kv'), 'tp'), parts along dimension 0
There are 2 independent parts, one for each index of `grp`. A program takes and returns all parts, laid end to end along the dimension named above; an argument that names none is the same for every part. Nothing has to cross between parts.
All inputs are finite; a program needn't handle non-finite values.
Results may differ from a plain program's by a relative error of at most 0.025.
Values may be sent and summed in bfloat16 or wider, within the bound.
No kernel may reach another device: no remote copies, remote signals or barrier semaphores. Data moves between devices by JAX's collectives and lax.ppermute only.
A program may use at most 64 MiB of HBM per device.

v0:
```python
import jax
import jax.numpy as jnp
from jax import lax
from jax.sharding import PartitionSpec as P

D = 4096
HEAD_DIM = 128
EPSILON = 1e-06


def l2_unit(values):
    return values * lax.rsqrt(jnp.sum(values * values, axis=-1, keepdims=True) + EPSILON)


def delta_update(query, key_vec, value_vec, log_decay, beta_gate, state):
    decayed = jnp.exp(log_decay)[..., None, None] * state
    recalled = jnp.einsum("shkv,shk->shv", decayed, key_vec, precision=lax.Precision.HIGHEST)
    update = beta_gate[..., None] * (value_vec - recalled)
    new_state = decayed + key_vec[..., :, None] * update[..., None, :]
    head_out = jnp.einsum("shkv,shk->shv", new_state, query, precision=lax.Precision.HIGHEST)
    return (new_state, head_out)


def head_mix(head_out, head_gain, z_gate):
    scaled = head_out * lax.rsqrt(jnp.mean(head_out * head_out, axis=-1, keepdims=True) + EPSILON)
    return (scaled * head_gain * jax.nn.silu(z_gate)).astype(jnp.bfloat16)


def local(
    stream,
    attn_gain,
    mlp_gain,
    w_query,
    w_key,
    w_value,
    w_zgate,
    w_decay,
    w_beta,
    decay_rate,
    head_gain,
    w_attn_out,
    w_gate,
    w_up,
    w_down,
    state,
):
    seq_count = state.shape[0]
    local_heads = state.shape[1]
    width = w_query.shape[1]
    heads_total = w_decay.shape[1]
    kv_offset = lax.axis_index("kv") * seq_count
    head_offset = lax.axis_index("tp") * local_heads
    block_rows = lax.all_gather(stream, "tp", axis=1, tiled=True).astype(jnp.float32)
    local_squares = jnp.sum(block_rows * block_rows, axis=1)
    normed = (block_rows * attn_gain.astype(jnp.float32)[None, :]).astype(jnp.bfloat16)
    small_weights = jnp.concatenate([w_decay, w_beta], axis=1)
    pieces = [
        jnp.dot(normed, weight, preferred_element_type=jnp.float32)
        for weight in (w_query, w_key, w_value, w_zgate)
    ]
    small = jnp.dot(normed, small_weights, preferred_element_type=jnp.float32)
    own_decay = lax.dynamic_slice_in_dim(small, head_offset, local_heads, 1)
    own_beta = lax.dynamic_slice_in_dim(small, heads_total + head_offset, local_heads, 1)
    summed = lax.psum_scatter(
        jnp.concatenate(pieces + [own_decay, own_beta], axis=1).astype(jnp.bfloat16),
        "kv",
        scatter_dimension=0,
        tiled=True,
    ).astype(jnp.float32)
    total_squares = lax.psum(local_squares, "kv")
    row_scale = lax.rsqrt(total_squares / D + EPSILON)
    own_scale = lax.dynamic_slice_in_dim(row_scale, kv_offset, seq_count, 0)
    summed = summed * own_scale[:, None]

    def head_block(index):
        return summed[:, index * width : (index + 1) * width].reshape(
            seq_count, local_heads, HEAD_DIM
        )

    query = l2_unit(head_block(0)) * HEAD_DIM ** (-0.5)
    key_vec = l2_unit(head_block(1))
    value_vec = head_block(2)
    z_gate = head_block(3)
    log_decay = -decay_rate[None, :] * jax.nn.softplus(
        summed[:, 4 * width : 4 * width + local_heads]
    )
    beta_gate = jax.nn.sigmoid(summed[:, 4 * width + local_heads :])
    new_state, head_out = delta_update(query, key_vec, value_vec, log_decay, beta_gate, state)
    mixed = head_mix(head_out, head_gain, z_gate).reshape(seq_count, width)
    attn_part = jnp.dot(
        lax.all_gather(mixed, "kv", axis=0, tiled=True),
        w_attn_out,
        preferred_element_type=jnp.float32,
    )
    attn_sum = lax.psum_scatter(
        attn_part.astype(jnp.bfloat16), "tp", scatter_dimension=1, tiled=True
    ).astype(jnp.float32)
    residual_stream = (stream.astype(jnp.float32) + attn_sum).astype(jnp.bfloat16)
    mlp_block = lax.all_gather(residual_stream, "tp", axis=1, tiled=True).astype(jnp.float32)
    mlp_local_squares = jnp.sum(mlp_block * mlp_block, axis=1)
    mlp_total_squares = lax.psum(mlp_local_squares, "kv")
    normed_mlp = (mlp_block * mlp_gain.astype(jnp.float32)[None, :]).astype(jnp.bfloat16)
    gate_part = jnp.dot(normed_mlp, w_gate, preferred_element_type=jnp.float32)
    up_part = jnp.dot(normed_mlp, w_up, preferred_element_type=jnp.float32)
    operands = (gate_part, up_part)
    totals = (
        lax.psum(operands[0].astype(jnp.bfloat16), "kv").astype(jnp.float32),
        lax.psum(operands[1].astype(jnp.bfloat16), "kv").astype(jnp.float32),
    )
    gate_sum, up_sum = (totals[0], totals[1])
    mlp_scale = lax.rsqrt(mlp_total_squares / D + EPSILON)
    hidden = (jax.nn.silu(gate_sum * mlp_scale[:, None]) * (up_sum * mlp_scale[:, None])).astype(
        jnp.bfloat16
    )
    down_part = jnp.dot(hidden, w_down, preferred_element_type=jnp.float32)
    mlp_sum = lax.psum_scatter(
        down_part.astype(jnp.bfloat16), "tp", scatter_dimension=1, tiled=True
    ).astype(jnp.float32)
    next_stream = (residual_stream.astype(jnp.float32) + mlp_sum).astype(jnp.bfloat16)
    return (next_stream, new_state)


def solution(mesh):
    return jax.shard_map(
        local,
        mesh=mesh,
        in_specs=(
            P("grp", ("kv", "tp")),
            P("kv"),
            P("kv"),
            P("kv", "tp"),
            P("kv", "tp"),
            P("kv", "tp"),
            P("kv", "tp"),
            P("kv", None),
            P("kv", None),
            P("tp"),
            P(),
            P("tp", "kv"),
            P("kv", "tp"),
            P("kv", "tp"),
            P("tp", "kv"),
            P(("grp", "kv"), "tp", None, None),
        ),
        out_specs=(P("grp", ("kv", "tp")), P(("grp", "kv"), "tp", None, None)),
        check_vma=False,
    )
```

profile of v0, /device:TPU:0, one launch (start us, length us, event | category | flops | bytes accessed | tf_op | source)
XLA Modules:
  0.0 189.6 jit_solution(2436157586402226002)
XLA Ops:
  7.2 0.8 convert_element_type.66
  8.1 6.6 %all_gather.9 = bf16[16,1024]{1,0:T(8,128)(2,1)S(1)} all-gather(bf16[16,256]{1,0:T(8,128)(2,1)} %param.16), channel_id=1, replica_groups=mesh['grp'=2,'kv'=4,'tp'=4] {'tp'}, dimensions={1}, use_global_device_ids=true | all-gather | bytes 40960 | tf_op jit(solution)/shard_map/all_gather | solution.py:53
  14.7 0.4 convolution_convert_fusion.6
  15.1 0.4 convolution_convert_fusion.5
  15.5 0.8 copy-done.4
  16.3 0.4 convolution_convert_fusion.4
  16.7 0.3 copy-done.5
  17.0 0.4 convolution_convert_fusion.7
  17.4 0.1 fusion.3
  17.6 0.8 concatenate.8
  18.5 0.1 fusion.10
  18.6 12.4 %psum.28 = f32[16]{0:T(128)S(1)} all-reduce(f32[16]{0:T(128)S(1)} %fusion.10), channel_id=1, replica_groups=mesh['grp'=2,'kv'=4,'tp'=4] {'kv'}, use_global_device_ids=true, to_apply=%region_2.0 | all-reduce | flops 16 | bytes 128 | tf_op jit(solution)/shard_map/psum | solution.py:70
  31.0 0.6 dynamic-slice
  32.3 22.4 %all-reduce.5.cloned.1.call-done = bf16[16,4112]{1,0:T(8,128)(2,1)} async-done(((bf16[16,4112]{1,0:T(8,128)(2,1)}), bf16[16,4112]{1,0:T(8,128)(2,1)}) %all-reduce.5.cloned.1.call-update) | async-done | bytes 131600
  54.8 1.1 convert_multiply_fusion.4
  56.2 3.6 %fusion = f32[4,8,1,128]{3,2,1,0:T(1,128)S(1)} fusion(f32[4,8,128,1]{2,3,1,0:T(1,128)S(1)} %bitcast.62, f32[4,8,128,128]{3,2,1,0:T(8,128)} %param.31, f32[4,8]{1,0:T(4,128)S(1)} %get-tuple-element.9), kind=kOutput, calls=%fused_computation.3 | convolution fusion | flops 6815744 | bytes 2130048 | tf_op jit(solution)/shard_map/shkv,shk->shv/dot_general | solution.py:17
  59.9 0.7 multiply_add_fusion
  60.7 1.3 copy-done.2
  62.0 1.9 fusion.36
  64.1 13.1 %all-gather = bf16[4,4,1024]{2,1,0:T(4,128)(2,1)S(1)} all-gather(bf16[1,4,1024]{2,1,0:T(4,128)(2,1)S(1)} %reshape.59), channel_id=1, replica_groups=mesh['grp'=2,'kv'=4,'tp'=4] {'kv'}, dimensions={0}, use_global_device_ids=true | all-gather | bytes 40960 | tf_op jit(solution)/shard_map/all_gather | solution.py:91
  77.3 2.6 %convolution_convert_fusion.3 = bf16[16,1024]{1,0:T(8,128)(2,1)} fusion(bf16[16,1024]{1,0:T(8,128)(2,1)S(1)} %reshape.60, bf16[1024,1024]{1,0:T(8,128)(2,1)} %param.27), kind=kOutput, calls=%fused_computation.6 | convolution fusion | flops 33570816 | bytes 2162688 | tf_op jit(solution)/shard_map/dot_general | solution.py:90
  79.9 19.6 %reduce-scatter.3.cloned.1.call-done = bf16[16,256]{1,0:T(8,128)(2,1)} async-done(((bf16[16,1024]{1,0:T(8,128)(2,1)}), bf16[16,256]{1,0:T(8,128)(2,1)}) %reduce-scatter.3.cloned.1.call-update) | async-done | bytes 8208 | tf_op jit(solution)/shard_map/reduce_scatter | solution.py:95
  99.6 0.7 add_convert_fusion.1
  100.3 5.2 %all_gather.11 = bf16[16,1024]{1,0:T(8,128)(2,1)S(1)} all-gather(bf16[16,256]{1,0:T(8,128)(2,1)S(1)} %add_convert_fusion.1), channel_id=1, replica_groups=mesh['grp'=2,'kv'=4,'tp'=4] {'tp'}, dimensions={1}, use_global_device_ids=true | all-gather | bytes 40960 | tf_op jit(solution)/shard_map/all_gather | solution.py:99
  105.5 0.1 fusion.12
  105.6 11.7 %psum.30 = f32[16]{0:T(128)S(1)} all-reduce(f32[16]{0:T(128)S(1)} %fusion.12), channel_id=1, replica_groups=mesh['grp'=2,'kv'=4,'tp'=4] {'kv'}, use_global_device_ids=true, to_apply=%region_9.10 | all-reduce | flops 16 | bytes 128 | tf_op jit(solution)/shard_map/psum | solution.py:101
  117.3 4.1 %convolution_convert_fusion = bf16[16,2816]{1,0:T(8,128)(2,1)} fusion(bf16[1024,2816]{1,0:T(8,128)(2,1)} %param.29, bf16[16,1024]{1,0:T(8,128)(2,1)S(1)} %all_gather.11, f32[1024]{0:T(1024)S(1)} %convert_element_type.75), kind=kOutput, calls=%fused_computation | convolution fusion | flops 92368896 | bytes 5894144 | tf_op jit(solution)/shard_map/dot_general | solution.py:104
  121.4 4.1 %convolution_convert_fusion.1 = bf16[16,2816]{1,0:T(8,128)(2,1)} fusion(bf16[1024,2816]{1,0:T(8,128)(2,1)} %param.28, bf16[16,1024]{1,0:T(8,128)(2,1)S(1)} %all_gather.11, f32[1024]{0:T(1024)S(1)} %convert_element_type.75), kind=kOutput, calls=%fused_computation.1 | convolution fusion | flops 92368896 | bytes 5894144 | tf_op jit(solution)/shard_map/dot_general | solution.py:103
  125.7 32.1 %all-reduce.7.cloned.1.call-done = (bf16[16,2816]{1,0:T(8,128)(2,1)}, bf16[16,2816]{1,0:T(8,128)(2,1)}) async-done(((bf16[16,2816]{1,0:T(8,128)(2,1)}, bf16[16,2816]{1,0:T(8,128)(2,1)}), (bf16[16,2816]{1,0:T(8,128)(2,1)}, bf16[16,2816]{1,0:T(8,128)(2,1)})) %all-reduce.7.cloned.1.call-update) | async-done | bytes 180240 | tf_op jit(solution)/shard_map/psum | solution.py:108
  157.7 4.3 %convolution_convert_fusion.2 = bf16[16,1024]{1,0:T(8,128)(2,1)} fusion(bf16[2816,1024]{1,0:T(8,128)(2,1)} %param.30, bf16[16,2816]{1,0:T(8,128)(2,1)} %get-tuple-element.2, bf16[16,2816]{1,0:T(8,128)(2,1)} %get-tuple-element.3, f32[16]{0:T(128)S(1)} %add_rsqrt_fusion.3), kind=kOutput, calls=%fused_computation.5 | convolution fusion | flops 92741632 | bytes 5980224 | tf_op jit(solution)/shard_map/dot_general | solution.py:115
  162.0 19.8 %reduce-scatter.5.cloned.1.call-done = bf16[16,256]{1,0:T(8,128)(2,1)} async-done(((bf16[16,1024]{1,0:T(8,128)(2,1)}), bf16[16,256]{1,0:T(8,128)(2,1)}) %reduce-scatter.5.cloned.1.call-update) | async-done | bytes 8208 | tf_op jit(solution)/shard_map/reduce_scatter | solution.py:116
  181.8 1.3 add_convert_fusion
  (50 shorter events, 1.1 us)
Async XLA Ops:
  7.2 7.5 %copy-start = (bf16[1024,1024]{1,0:T(8,128)(2,1)S(1)}, bf16[1024,1024]{1,0:T(8,128)(2,1)}, u32[]{:S(2)}) copy-start(bf16[1024,1024]{1,0:T(8,128)(2,1)} %param.20) | copy-start | bytes 6291460
  7.2 47.6 %all-reduce.5.cloned.1.call-start = ((), (), s32[]{:S(2)}) async-start(), calls=%async_computation.4 | async-start | bytes 270336
  7.2 7.8 %copy-start.3 = (bf16[1024,1024]{1,0:T(8,128)(2,1)S(1)}, bf16[1024,1024]{1,0:T(8,128)(2,1)}, u32[]{:S(2)}) copy-start(bf16[1024,1024]{1,0:T(8,128)(2,1)} %param.21) | copy-start | bytes 6291460
  14.7 1.6 copy-start.4
  15.1 1.9 %copy-start.5 = (bf16[1024,1024]{1,0:T(8,128)(2,1)S(1)}, bf16[1024,1024]{1,0:T(8,128)(2,1)}, u32[]{:S(2)}) copy-start(bf16[1024,1024]{1,0:T(8,128)(2,1)} %param.19) | copy-start | bytes 6291460
  16.3 1.1 copy-start.9
  16.3 1.1 copy-start.10
  16.3 2.3 %copy-start.11 = (f32[8]{0:T(128)S(1)}, f32[8]{0:T(128)}, u32[]{:S(2)}) copy-start(f32[8]{0:T(128)} %param.25) | copy-start | bytes 100
  16.3 14.7 %copy-start.12 = (u32[32]{0:T(128)S(1)}, u32[32]{0:T(128)}, u32[]{:S(2)}) copy-start(u32[32]{0:T(128)} %constant.46) | copy-start | bytes 388
  18.4 81.2 %reduce-scatter.3.cloned.1.call-start = ((), (), s32[]{:S(2)}) async-start(), calls=%async_computation.2 | async-start | bytes 40960 | tf_op jit(solution)/shard_map/reduce_scatter | solution.py:95
  54.8 5.2 %copy-start.1 = (f32[4,8,128,128]{3,2,1,0:T(8,128)S(1)}, f32[4,8,128,128]{3,2,1,0:T(8,128)}, u32[]{:S(2)}) copy-start(f32[4,8,128,128]{3,2,1,0:T(8,128)} %param.31) | copy-start | bytes 6291460
  60.7 1.3 copy-start.2
  60.7 3.3 %copy-start.8 = (f32[128]{0:T(128)S(1)}, f32[128]{0:T(128)}, u32[]{:S(2)}) copy-start(f32[128]{0:T(128)} %param.26) | copy-start | bytes 1540
  62.0 17.9 %copy-start.7 = (bf16[1024]{0:T(1024)(128)(2,1)S(1)}, bf16[1024]{0:T(1024)(128)(2,1)}, u32[]{:S(2)}) copy-start(bf16[1024]{0:T(1024)(128)(2,1)} %param.18) | copy-start | bytes 6148
  62.0 37.6 %copy-start.6 = (bf16[16,256]{1,0:T(8,128)(2,1)S(1)}, bf16[16,256]{1,0:T(8,128)(2,1)}, u32[]{:S(2)}) copy-start(bf16[16,256]{1,0:T(8,128)(2,1)} %param.16) | copy-start | bytes 24580
  79.9 77.9 %all-reduce.7.cloned.1.call-start = ((), (), s32[]{:S(2)}) async-start(), calls=%async_computation.5 | async-start | bytes 360448 | tf_op jit(solution)/shard_map/psum | solution.py:108
  125.6 56.2 %reduce-scatter.5.cloned.1.call-start = ((), (), s32[]{:S(2)}) async-start(), calls=%async_computation.3 | async-start | bytes 40960 | tf_op jit(solution)/shard_map/reduce_scatter | solution.py:116
Sparse Core Ops, SparseCore 0:
  18.5 36.2 all-reduce.4
  80.0 19.5 reduce-scatter.2
  125.7 31.9 all-reduce.6
  162.1 19.5 reduce-scatter.4
where the time goes:
time: 190 us
  waiting for transfers between devices  94 us (49%)
  blocking collectives  49 us (26%)
  matrix products  22.3 us (12%)
  between operations  14.6 us (8%)
  other arithmetic  5.53 us (3%)
  local copies, waits for them, and re-layouts  4.03 us (2%)
    psum x1, waiting for transfers between devices, local(): lax.psum(operands[1].astype(jnp.bfloat16), 'kv').astype(jnp.float32)  32.1 us
    unnamed x5, waiting for transfers between devices  22.5 us
    reduce_scatter x1, waiting for transfers between devices, local(): lax.psum_scatter(down_part.astype(jnp.bfloat16), 'tp', scatter_dimension=...  19.8 us
    reduce_scatter x1, waiting for transfers between devices, local(): lax.psum_scatter(attn_part.astype(jnp.bfloat16), 'tp', scatter_dimension=...  19.6 us
    all_gather x1, blocking collectives, local(): lax.all_gather(mixed, 'kv', axis=0, tiled=True)  13.1 us
    psum x1, blocking collectives, local(): total_squares = lax.psum(local_squares, 'kv')  12.4 us
    psum x1, blocking collectives, local(): mlp_total_squares = lax.psum(mlp_local_squares, 'kv')  11.7 us
    all_gather x1, blocking collectives, local(): lax.all_gather(stream, 'tp', axis=1, tiled=True).astype(jnp.float32)  6.6 us
  transfers between devices with their start and end apart: 4, of which 4 were waited for; matrix products, arithmetic and copies ran while one was open for 0% of the time, Pallas kernels for 0%

commit v1 on v0

--- a/solution.py
+++ b/solution.py
@@ -44,6 +44,10 @@
     w_down,
     state,
 ):
+
+    def _find_vectors(t0):
+        return jnp.sum(jax.lax.all_gather(t0, "kv"), axis=0)
+
     seq_count = state.shape[0]
     local_heads = state.shape[1]
     width = w_query.shape[1]
@@ -105,7 +109,7 @@
     operands = (gate_part, up_part)
     totals = (
         lax.psum(operands[0].astype(jnp.bfloat16), "kv").astype(jnp.float32),
-        lax.psum(operands[1].astype(jnp.bfloat16), "kv").astype(jnp.float32),
+        _find_vectors(operands[1].astype(jnp.bfloat16)).astype(jnp.float32),
     )
     gate_sum, up_sum = (totals[0], totals[1])
     mlp_scale = lax.rsqrt(mlp_total_squares / D + EPSILON)

time: 190 us -> 180 us (0.947)
  waiting for transfers between devices: 94 us -> 70.5 us
  blocking collectives: 49 us -> 63.2 us
    psum x1, waiting for transfers between devices: 32.1 us -> 8.59 us  [local(): lax.psum(operands[0].astype(jnp.bfloat16), 'kv').astype(jnp.float32)]
    all_gather x0 -> x1, blocking collectives: none -> 14.1 us  [_find_vectors(): return jnp.sum(jax.lax.all_gather(t0, 'kv'), axis=0)]
where the time goes in v1:
time: 180 us; the launch traced here: 179 us
  waiting for transfers between devices  70.5 us (39%)
  blocking collectives  63.2 us (35%)
  matrix products  21.6 us (12%)
  between operations  14.6 us (8%)
  other arithmetic  5.43 us (3%)
  local copies, waits for them, and re-layouts  3.95 us (2%)
    unnamed x5, waiting for transfers between devices  22.5 us
    reduce_scatter x1, waiting for transfers between devices, local(): lax.psum_scatter(down_part.astype(jnp.bfloat16), 'tp', scatter_dimension=...  19.7 us
    reduce_scatter x1, waiting for transfers between devices, local(): lax.psum_scatter(attn_part.astype(jnp.bfloat16), 'tp', scatter_dimension=...  19.6 us
    all_gather x1, blocking collectives, _find_vectors(): return jnp.sum(jax.lax.all_gather(t0, 'kv'), axis=0)  14.1 us
    all_gather x1, blocking collectives, local(): lax.all_gather(mixed, 'kv', axis=0, tiled=True)  13.1 us
    psum x1, blocking collectives, local(): total_squares = lax.psum(local_squares, 'kv')  12.4 us
    psum x1, blocking collectives, local(): mlp_total_squares = lax.psum(mlp_local_squares, 'kv')  11.8 us
    psum x1, waiting for transfers between devices, local(): lax.psum(operands[0].astype(jnp.bfloat16), 'kv').astype(jnp.float32)  8.59 us
  transfers between devices with their start and end apart: 4, of which 4 were waited for; matrix products, arithmetic and copies ran while one was open for 0% of the time, Pallas kernels for 0%

profile of v1, /device:TPU:0, one launch (start us, length us, event | category | flops | bytes accessed | tf_op | source)
XLA Modules:
  0.0 179.4 jit_solution(9377656124833021262)
XLA Ops:
  7.2 6.6 %all_gather.15 = bf16[16,1024]{1,0:T(8,128)(2,1)S(1)} all-gather(bf16[16,256]{1,0:T(8,128)(2,1)} %param.16), channel_id=1, replica_groups=mesh['grp'=2,'kv'=4,'tp'=4] {'tp'}, dimensions={1}, use_global_device_ids=true | all-gather | bytes 40960 | tf_op jit(solution)/shard_map/all_gather | solution.py:57
  13.9 0.7 convert_element_type.68
  14.5 0.4 convolution_convert_fusion.4
  14.9 0.4 convolution_convert_fusion.5
  15.3 0.8 copy-done.4
  16.1 0.4 convolution_convert_fusion.6
  16.5 0.3 copy-done.5
  16.9 0.4 convolution_convert_fusion.7
  17.3 0.1 fusion.3
  17.5 0.8 concatenate.8
  18.3 0.1 fusion.10
  18.4 12.4 %psum.21 = f32[16]{0:T(128)S(1)} all-reduce(f32[16]{0:T(128)S(1)} %fusion.10), channel_id=1, replica_groups=mesh['grp'=2,'kv'=4,'tp'=4] {'kv'}, use_global_device_ids=true, to_apply=%region_2.0 | all-reduce | flops 16 | bytes 128 | tf_op jit(solution)/shard_map/psum | solution.py:74
  30.9 0.6 dynamic-slice
  32.2 22.5 %all-reduce.6.cloned.1.call-done = bf16[16,4112]{1,0:T(8,128)(2,1)} async-done(((bf16[16,4112]{1,0:T(8,128)(2,1)}), bf16[16,4112]{1,0:T(8,128)(2,1)}) %all-reduce.6.cloned.1.call-update) | async-done | bytes 131600
  54.7 1.1 convert_multiply_fusion.4
  56.0 3.6 %fusion = f32[4,8,1,128]{3,2,1,0:T(1,128)S(1)} fusion(f32[4,8,128,1]{2,3,1,0:T(1,128)S(1)} %bitcast.64, f32[4,8,128,128]{3,2,1,0:T(8,128)} %param.31, f32[4,8]{1,0:T(4,128)S(1)} %get-tuple-element.7), kind=kOutput, calls=%fused_computation.3 | convolution fusion | flops 6815744 | bytes 2130048 | tf_op jit(solution)/shard_map/shkv,shk->shv/dot_general | solution.py:17
  59.7 0.8 multiply_add_fusion
  60.6 1.2 copy-done.2
  61.8 1.9 %fusion.36 = f32[4,8,1,128]{3,2,1,0:T(1,128)S(1)} fusion(f32[4,8,128,128]{3,2,1,0:T(8,128)S(1)} %multiply_add_fusion, f32[4,8,128,1]{2,3,1,0:T(1,128)S(1)} %bitcast.68), kind=kOutput, calls=%fused_computation.67 | convolution fusion | flops 6291456 | bytes 2129920 | tf_op jit(solution)/shard_map/shkv,shk->shv/dot_general | solution.py:20
  63.9 13.1 %all-gather.1 = bf16[4,4,1024]{2,1,0:T(4,128)(2,1)S(1)} all-gather(bf16[1,4,1024]{2,1,0:T(4,128)(2,1)S(1)} %reshape.60), channel_id=1, replica_groups=mesh['grp'=2,'kv'=4,'tp'=4] {'kv'}, dimensions={0}, use_global_device_ids=true | all-gather | bytes 40960 | tf_op jit(solution)/shard_map/all_gather | solution.py:95
  77.1 2.6 %convolution_convert_fusion.3 = bf16[16,1024]{1,0:T(8,128)(2,1)} fusion(bf16[16,1024]{1,0:T(8,128)(2,1)S(1)} %reshape.61, bf16[1024,1024]{1,0:T(8,128)(2,1)} %param.27), kind=kOutput, calls=%fused_computation.6 | convolution fusion | flops 33570816 | bytes 2162688 | tf_op jit(solution)/shard_map/dot_general | solution.py:94
  79.7 19.6 %reduce-scatter.3.cloned.1.call-done = bf16[16,256]{1,0:T(8,128)(2,1)} async-done(((bf16[16,1024]{1,0:T(8,128)(2,1)}), bf16[16,256]{1,0:T(8,128)(2,1)}) %reduce-scatter.3.cloned.1.call-update) | async-done | bytes 8208 | tf_op jit(solution)/shard_map/reduce_scatter | solution.py:99
  99.4 0.7 add_convert_fusion.1
  100.1 5.2 %all_gather.17 = bf16[16,1024]{1,0:T(8,128)(2,1)S(1)} all-gather(bf16[16,256]{1,0:T(8,128)(2,1)S(1)} %add_convert_fusion.1), channel_id=1, replica_groups=mesh['grp'=2,'kv'=4,'tp'=4] {'tp'}, dimensions={1}, use_global_device_ids=true | all-gather | bytes 40960 | tf_op jit(solution)/shard_map/all_gather | solution.py:103
  105.4 3.5 %convolution_convert_fusion = bf16[16,2816]{1,0:T(8,128)(2,1)S(1)} fusion(bf16[1024,2816]{1,0:T(8,128)(2,1)} %param.29, bf16[16,1024]{1,0:T(8,128)(2,1)S(1)} %all_gather.17, f32[1024]{0:T(1024)S(1)} %convert_element_type.77), kind=kOutput, calls=%fused_computation | convolution fusion | flops 92368896 | bytes 5894144 | tf_op jit(solution)/shard_map/dot_general | solution.py:108
  108.9 4.1 %convolution_convert_fusion.1 = bf16[16,2816]{1,0:T(8,128)(2,1)} fusion(bf16[1024,2816]{1,0:T(8,128)(2,1)} %param.28, bf16[16,1024]{1,0:T(8,128)(2,1)S(1)} %all_gather.17, f32[1024]{0:T(1024)S(1)} %convert_element_type.77), kind=kOutput, calls=%fused_computation.1 | convolution fusion | flops 92368896 | bytes 5894144 | tf_op jit(solution)/shard_map/dot_general | solution.py:107
  113.1 11.8 %psum.23 = f32[16]{0:T(128)S(1)} all-reduce(f32[16]{0:T(128)S(1)} %fusion.12), channel_id=1, replica_groups=mesh['grp'=2,'kv'=4,'tp'=4] {'kv'}, use_global_device_ids=true, to_apply=%region_9.10 | all-reduce | flops 16 | bytes 128 | tf_op jit(solution)/shard_map/psum | solution.py:105
  124.8 14.1 %all-gather = bf16[64,2816]{1,0:T(8,128)(2,1)S(1)} all-gather(bf16[16,2816]{1,0:T(8,128)(2,1)S(1)} %convolution_convert_fusion), channel_id=2, replica_groups=mesh['grp'=2,'kv'=4,'tp'=4] {'kv'}, dimensions={0}, use_global_device_ids=true | all-gather | bytes 450560 | tf_op jit(solution)/shard_map/all_gather | solution.py:49
  139.0 8.6 %all-reduce.4.cloned.1.call-done = bf16[16,2816]{1,0:T(8,128)(2,1)} async-done(((bf16[16,2816]{1,0:T(8,128)(2,1)}), bf16[16,2816]{1,0:T(8,128)(2,1)}) %all-reduce.4.cloned.1.call-update) | async-done | bytes 90128 | tf_op jit(solution)/shard_map/psum | solution.py:111
  147.6 4.2 %convolution_convert_fusion.2 = bf16[16,1024]{1,0:T(8,128)(2,1)} fusion(bf16[2816,1024]{1,0:T(8,128)(2,1)} %param.30, bf16[16,2816]{1,0:T(8,128)(2,1)S(1)} %reduce_sum.62, bf16[16,2816]{1,0:T(8,128)(2,1)} %all-reduce.4.cloned.1.call-done, f32[16]{0:T(128)S(1)} %add_rsqrt_fusion.3), kind=kOutput, calls=%fused_computation.5 | convolution fusion | flops 92741632 | bytes 5980224 | tf_op jit(solution)/shard_map/dot_general | solution.py:119
  151.8 19.7 %reduce-scatter.5.cloned.1.call-done = bf16[16,256]{1,0:T(8,128)(2,1)} async-done(((bf16[16,1024]{1,0:T(8,128)(2,1)}), bf16[16,256]{1,0:T(8,128)(2,1)}) %reduce-scatter.5.cloned.1.call-update) | async-done | bytes 8208 | tf_op jit(solution)/shard_map/reduce_scatter | solution.py:120
  171.6 1.3 add_convert_fusion
  (52 shorter events, 1.3 us)
Async XLA Ops:
  7.2 7.4 %copy-start = (bf16[1024,1024]{1,0:T(8,128)(2,1)S(1)}, bf16[1024,1024]{1,0:T(8,128)(2,1)}, u32[]{:S(2)}) copy-start(bf16[1024,1024]{1,0:T(8,128)(2,1)} %param.22) | copy-start | bytes 6291460
  7.2 47.5 %all-reduce.6.cloned.1.call-start = ((), (), s32[]{:S(2)}) async-start(), calls=%async_computation.5 | async-start | bytes 270336
  7.2 7.7 %copy-start.3 = (bf16[1024,1024]{1,0:T(8,128)(2,1)S(1)}, bf16[1024,1024]{1,0:T(8,128)(2,1)}, u32[]{:S(2)}) copy-start(bf16[1024,1024]{1,0:T(8,128)(2,1)} %param.21) | copy-start | bytes 6291460
  14.5 1.6 copy-start.4
  14.9 1.9 %copy-start.5 = (bf16[1024,1024]{1,0:T(8,128)(2,1)S(1)}, bf16[1024,1024]{1,0:T(8,128)(2,1)}, u32[]{:S(2)}) copy-start(bf16[1024,1024]{1,0:T(8,128)(2,1)} %param.19) | copy-start | bytes 6291460
  16.1 1.1 copy-start.9
  16.1 1.1 copy-start.10
  16.1 14.7 %copy-start.11 = (f32[8]{0:T(128)S(1)}, f32[8]{0:T(128)}, u32[]{:S(2)}) copy-start(f32[8]{0:T(128)} %param.25) | copy-start | bytes 100
  16.1 14.8 %copy-start.12 = (u32[32]{0:T(128)S(1)}, u32[32]{0:T(128)}, u32[]{:S(2)}) copy-start(u32[32]{0:T(128)} %constant.48) | copy-start | bytes 388
  18.3 81.1 %reduce-scatter.3.cloned.1.call-start = ((), (), s32[]{:S(2)}) async-start(), calls=%async_computation.2 | async-start | bytes 40960 | tf_op jit(solution)/shard_map/reduce_scatter | solution.py:99
  54.7 5.1 %copy-start.1 = (f32[4,8,128,128]{3,2,1,0:T(8,128)S(1)}, f32[4,8,128,128]{3,2,1,0:T(8,128)}, u32[]{:S(2)}) copy-start(f32[4,8,128,128]{3,2,1,0:T(8,128)} %param.31) | copy-start | bytes 6291460
  60.5 1.3 copy-start.2
  60.5 3.3 %copy-start.8 = (f32[128]{0:T(128)S(1)}, f32[128]{0:T(128)}, u32[]{:S(2)}) copy-start(f32[128]{0:T(128)} %param.26) | copy-start | bytes 1540
  61.8 17.9 %copy-start.7 = (bf16[1024]{0:T(1024)(128)(2,1)S(1)}, bf16[1024]{0:T(1024)(128)(2,1)}, u32[]{:S(2)}) copy-start(bf16[1024]{0:T(1024)(128)(2,1)} %param.18) | copy-start | bytes 6148
  61.8 37.6 %copy-start.6 = (bf16[16,256]{1,0:T(8,128)(2,1)S(1)}, bf16[16,256]{1,0:T(8,128)(2,1)}, u32[]{:S(2)}) copy-start(bf16[16,256]{1,0:T(8,128)(2,1)} %param.16) | copy-start | bytes 24580
  79.7 67.9 %all-reduce.4.cloned.1.call-start = ((), (), s32[]{:S(2)}) async-start(), calls=%async_computation.3 | async-start | bytes 180224 | tf_op jit(solution)/shard_map/psum | solution.py:111
  113.0 58.5 %reduce-scatter.5.cloned.1.call-start = ((), (), s32[]{:S(2)}) async-start(), calls=%async_computation.4 | async-start | bytes 40960 | tf_op jit(solution)/shard_map/reduce_scatter | solution.py:120
Sparse Core Ops, SparseCore 0:
  18.4 36.2 all-reduce.5
  79.8 19.5 reduce-scatter.2
  113.1 34.4 all-reduce.3
  152.0 19.5 reduce-scatter.4
